TPU v7x, 512 devices: a whole 4x4x16 slice. The times are simulated.
512 devices in a mesh: sp: 128 (over z, x, core), tp: 4 (over y).
Axes of the slice: x: 4, y: 4, z: 16, core: 2. Of those that a mesh axis runs over, the one named last changes fastest.
Arguments:
- tokens: bfloat16 [49152, 2048], P('sp'), may hold values from -6 to 6
- doc_ids: int32 [49152], P('sp'), may hold values from 0 to 31, never falling along the last dimension, each value on 1 to 3072 neighbouring positions
- pre_gain: float32 [2, 2048], replicated, may hold values from 0.1 to 1.9
- value_proj: bfloat16 [2, 2048, 1024], P(None, 'sp', 'tp'), may hold values from -0.5 to 0.5
- gate_proj: bfloat16 [2, 2048, 1024], P(None, 'sp', 'tp'), may hold values from -0.5 to 0.5
- out_proj: bfloat16 [2, 1024, 2048], P(None, 'tp', 'sp'), may hold values from -0.1875 to 0.1875
- conv_taps: float32 [2, 31, 1024], P(None, None, 'tp'), may hold values from -2.2 to 2.2
- norm_gain: float32 [2, 1024], P(None, 'tp'), may hold values from 0.1 to 1.9
- norm_shift: float32 [2, 1024], P(None, 'tp'), may hold values from -3 to 3
Outputs:
- hidden: bfloat16 [49152, 2048], P('sp')
Inputs may be any that keep to these rules, and one draw needn't show every extreme that they name: `doc_ids`: document numbers never fall along the sequence; each document has 1 to 3072 positions.
All inputs are finite; a program needn't handle non-finite values.
Results may differ from a plain program's by a relative error of at most 0.017.
Values may be sent and summed in bfloat16 or wider, within the bound.
A program may use at most 64 MiB of HBM per device.

v0:
```python
import jax
import jax.numpy as jnp
from jax import lax
from jax.sharding import PartitionSpec as P

epsilon = 1e-06


def rows_first(arrays, axis, dims):
    turned = [jnp.moveaxis(a, dim, 0) for a, dim in zip(arrays, dims)]
    both = jnp.concatenate([t.reshape(len(t), -1) for t in turned], axis=1)
    out, at, outs = (lax.all_gather(both, axis, axis=0, tiled=True), 0, [])
    for t, dim in zip(turned, dims):
        slab = out[:, at : at + t[0].size].reshape(-1, *t.shape[1:])
        outs.append(jnp.moveaxis(slab, 0, dim))
        at += t[0].size
    return tuple(outs)


def passed_along(value, axis, steps):
    count = lax.axis_size(axis)
    first, last = (max(0, -steps), min(count, count - steps))
    return lax.ppermute(value, axis, [(source, source + steps) for source in range(first, last)])


def sent_to_all(value, axis):
    copies = jnp.broadcast_to(value, (lax.axis_size(axis), *value.shape))
    return lax.all_to_all(copies, axis, split_axis=0, concat_axis=0, tiled=True)


def taken_together(value, axis):
    everything = sent_to_all(value, axis)
    return jnp.sum(everything, axis=0)


def together(arrays, axis):
    ravelled, at, outs = (jnp.concatenate([a.reshape(-1) for a in arrays]), 0, [])
    total = taken_together(ravelled, axis)
    for a in arrays:
        outs.append(total[at : at + a.size].reshape(a.shape))
        at += a.size
    return tuple(outs)


def cut_along(value, dim, length):
    before, after = (value.shape[:dim], value.shape[dim + 1 :])
    return jnp.moveaxis(value.reshape(*before, length, -1, *after), dim, 0)


def summed_on_arrival(value, axis, dim):
    pieces = cut_along(value, dim, lax.axis_size(axis))
    arrived = lax.all_to_all(pieces, axis, split_axis=0, concat_axis=0, tiled=True)
    return arrived.astype(jnp.float32).sum(axis=0)


def in_order(pieces, dim):
    lengths = list(pieces.shape[1:])
    lengths[dim] *= pieces.shape[0]
    return jnp.moveaxis(pieces, 0, dim).reshape(lengths)


def collect(value, axis, dim):
    return in_order(sent_to_all(value, axis), dim)


def on_device(
    tokens, doc_ids, pre_gain, value_proj, gate_proj, out_proj, conv_taps, norm_gain, norm_shift
):
    layer_count = value_proj.shape[0]
    tap_count = conv_taps.shape[1]
    reach_rows = tap_count - 1
    row_count = tokens.shape[0]
    block_width = conv_taps.shape[2]
    channels = block_width * lax.axis_size("tp")
    hidden = tokens
    full_value, full_gate, full_out = rows_first((value_proj, gate_proj, out_proj), "sp", (1, 1, 2))
    for layer_index in range(layer_count):
        wide_state = hidden.astype(jnp.float32)
        scale = lax.rsqrt(jnp.mean(wide_state * wide_state, axis=-1, keepdims=True) + epsilon)
        normed = (wide_state * scale * pre_gain[layer_index]).astype(jnp.bfloat16)
        value_acc = jnp.dot(normed, full_value[layer_index], preferred_element_type=jnp.float32)
        gate_acc = jnp.dot(normed, full_gate[layer_index], preferred_element_type=jnp.float32)
        value_half = value_acc.astype(jnp.bfloat16)
        gate_half = gate_acc.astype(jnp.bfloat16)
        gated_rows = (
            value_half.astype(jnp.float32) * jax.nn.sigmoid(gate_half.astype(jnp.float32))
        ).astype(jnp.bfloat16)
        prev_rows, prev_docs = passed_along(
            (gated_rows[row_count - reach_rows :], doc_ids[row_count - reach_rows :]), "sp", 1
        )
        padded = jnp.concatenate([prev_rows, gated_rows]).astype(jnp.float32)
        padded_docs = jnp.concatenate([prev_docs, doc_ids])
        conv_out = jnp.zeros((row_count, block_width), jnp.float32)
        for offset in range(tap_count):
            first_row = reach_rows - offset
            same_doc = (padded_docs[first_row : first_row + row_count] == doc_ids)[:, None]
            term = (
                conv_taps[layer_index, offset][None, :] * padded[first_row : first_row + row_count]
            )
            conv_out = conv_out + jnp.where(same_doc, term, jnp.float32(0.0))
        row_sums, square_sums = together(
            (jnp.sum(conv_out, axis=1), jnp.sum(conv_out * conv_out, axis=1)), "tp"
        )
        row_mean = (row_sums / channels)[:, None]
        row_var = (square_sums / channels)[:, None] - row_mean * row_mean
        normalized = (
            norm_gain[layer_index] * (conv_out - row_mean) * lax.rsqrt(row_var + epsilon)
            + norm_shift[layer_index]
        )
        activated = jax.nn.silu(normalized).astype(jnp.bfloat16)
        partial_value = jnp.dot(
            activated, full_out[layer_index], preferred_element_type=jnp.float32
        )
        summed = summed_on_arrival(partial_value.astype(jnp.bfloat16), "tp", 1)
        branch = summed.astype(jnp.bfloat16)
        piece_width = summed.shape[1]
        own_cols = lax.dynamic_slice_in_dim(
            hidden, lax.axis_index("tp") * piece_width, piece_width, 1
        )
        updated = (own_cols.astype(jnp.float32) + branch.astype(jnp.float32)).astype(jnp.bfloat16)
        hidden = collect(updated, "tp", 1)
    return hidden


def solution(mesh):
    return jax.shard_map(
        on_device,
        mesh=mesh,
        in_specs=(
            P("sp", None),
            P("sp"),
            P(),
            P(None, "sp", "tp"),
            P(None, "sp", "tp"),
            P(None, "tp", "sp"),
            P(None, None, "tp"),
            P(None, "tp"),
            P(None, "tp"),
        ),
        out_specs=P("sp", None),
        check_vma=False,
    )
```

profile of v0, /device:TPU:1, one launch (start us, length us, event | category | flops | bytes accessed | tf_op | source)
XLA Modules:
  0.0 310.0 jit_solution(1334254646113636902)
XLA Ops:
  6.5 0.7 copy.87
  7.3 0.7 copy.88
  8.0 0.7 copy.86
  8.7 0.6 pad_maximum_fusion
  9.3 0.8 slice.568
  10.1 4.5 %collective-permute-start.1 = (s32[30]{0:T(128)S(1)}, s32[30]{0:T(128)S(1)}, u32[]{:S(2)}, u32[]{:S(2)}) collective-permute-start(s32[30]{0:T(128)S(1)} %slice.568), channel_id=1, source_target_pairs={{0,4},{4,8},{8,12},{12,16},{16,20},{20,24},{24,28},{28,32},{32,36}... | collective-permute-start | bytes 368 | tf_op jit(solution)/shard_map/ppermute | solution.py:23
  14.6 1.8 fusion
  16.4 0.8 fusion.164
  17.2 0.9 fusion.163
  18.0 0.9 fusion.162
  18.9 0.8 slice_reduce_fusion
  19.7 0.8 fusion.165
  20.5 0.8 pad_add_fusion
  21.3 0.8 slice_compare_fusion.29
  22.0 138.2 %all-gather.2.cloned.1.call-done = bf16[2048,1536]{1,0:T(8,128)(2,1)} async-done(((bf16[16,1536]{1,0:T(8,128)(2,1)}), bf16[2048,1536]{1,0:T(8,128)(2,1)}) %all-gather.2.cloned.1.call-update) | async-done | bytes 6291472 | tf_op jit(solution)/shard_map/all_gather | solution.py:12
  160.2 3.4 %fusion.160 = (bf16[2048,512]{1,0:T(8,128)(2,1)S(1)}, bf16[2048,512]{1,0:T(8,128)(2,1)S(1)}, bf16[2048,512]{1,0:T(8,128)(2,1)S(1)}) fusion(bf16[2048,1536]{1,0:T(8,128)(2,1)} %all-gather.2.cloned.1.call-done), kind=kLoop, calls=%fused_computation.288 | loop fusion | bytes 12582912 | tf_op jit(solution)/shard_map/slice | solution.py:14
  164.0 1.1 copy-done
  165.1 1.3 copy-done.2
  166.4 0.6 fusion.21
  167.0 0.6 fusion.20
  167.7 2.1 collective-permute-start
  169.9 0.9 collective-permute-done
  170.9 3.3 %fusion.157 = (f32[384]{0:T(512)S(1)}, f32[384]{0:T(512)S(1)}, f32[384,256]{1,0:T(8,128)S(1)}) fusion(f32[414,256]{1,0:T(8,128)S(1)} %maximum_convert_fusion, f32[256]{0:T(256)S(1)} %bitcast.193, pred[384]{0:T(512)(128)(4,1)S(1)} %get-tuple-element.110, f32[256]{0:T(256)S(1)} %bitcast.194, pred[384]{0:T(512)(128)(4,1)S(1)} %get-tuple-element.111, ...), kind=kLoop, calls=%fused_computation.287 | loop fusion | flops 9239808 | bytes 12629248 | tf_op jit(solution)/shard_map/reduce_sum | solution.py:102
  174.8 4.0 %all-to-all-start = ((f32[4,1,768]{2,1,0:T(1,128)}), f32[4,1,768]{2,1,0:T(1,128)S(1)}, u32[]{:S(2)}, u32[]{:S(2)}) async-start(f32[4,1,768]{2,1,0:T(1,128)} %broadcast_in_dim.423), calls=%async_computation | async-start | bytes 24576 | tf_op jit(solution)/shard_map/all_to_all | solution.py:28
  178.8 2.5 copy.74
  181.3 1.7 all-to-all-done
  183.0 1.9 convolution_convert_fusion.1
  184.9 1.3 copy.96
  186.2 3.6 %all-to-all-start.1 = ((bf16[4,384,512]{2,1,0:T(8,128)(2,1)}), bf16[4,384,512]{2,1,0:T(8,128)(2,1)S(1)}, u32[]{:S(2)}, u32[]{:S(2)}) async-start(bf16[4,384,512]{2,1,0:T(8,128)(2,1)} %bitcast.135), calls=%async_computation.1 | async-start | bytes 3145728 | tf_op jit(solution)/shard_map/all_to_all | solution.py:52
  189.8 19.2 %all-to-all-done.1 = bf16[4,384,512]{2,1,0:T(8,128)(2,1)S(1)} async-done(((bf16[4,384,512]{2,1,0:T(8,128)(2,1)}), bf16[4,384,512]{2,1,0:T(8,128)(2,1)S(1)}, u32[]{:S(2)}, u32[]{:S(2)}) %all-to-all-start.1) | async-done | bytes 1572896 | tf_op jit(solution)/shard_map/all_to_all | solution.py:52
  209.4 1.1 add_convert_fusion.1
  210.5 1.3 broadcast_in_dim.424
  211.7 3.6 %all-to-all-start.2 = ((bf16[4,384,512]{2,1,0:T(8,128)(2,1)}), bf16[4,384,512]{2,1,0:T(8,128)(2,1)S(1)}, u32[]{:S(2)}, u32[]{:S(2)}) async-start(bf16[4,384,512]{2,1,0:T(8,128)(2,1)} %broadcast_in_dim.424), calls=%async_computation.2 | async-start | bytes 3145728 | tf_op jit(solution)/shard_map/all_to_all | solution.py:28
  215.3 18.3 %all-to-all-done.2 = bf16[4,384,512]{2,1,0:T(8,128)(2,1)S(1)} async-done(((bf16[4,384,512]{2,1,0:T(8,128)(2,1)}), bf16[4,384,512]{2,1,0:T(8,128)(2,1)S(1)}, u32[]{:S(2)}, u32[]{:S(2)}) %all-to-all-start.2) | async-done | bytes 1572896 | tf_op jit(solution)/shard_map/all_to_all | solution.py:28
  233.6 0.9 copy.68
  235.4 0.7 copy-done.1
  237.1 0.7 fusion.12
  237.8 4.3 %collective-permute-start.2 = (bf16[30,256]{1,0:T(8,128)(2,1)S(1)}, bf16[30,256]{1,0:T(8,128)(2,1)S(1)}, u32[]{:S(2)}, u32[]{:S(2)}) collective-permute-start(bf16[30,256]{1,0:T(8,128)(2,1)S(1)} %slice.775), channel_id=1, source_target_pairs={{0,4},{4,8},{8,12},{12,16},{16,20},{20,24},{24,28},{28,32},{32,36}... | collective-permute-start | bytes 46088 | tf_op jit(solution)/shard_map/ppermute | solution.py:23
  242.1 0.9 fusion.161
  243.1 3.3 %fusion.156 = (f32[384]{0:T(512)S(1)}, f32[384]{0:T(512)S(1)}, f32[384,256]{1,0:T(8,128)S(1)}) fusion(f32[414,256]{1,0:T(8,128)S(1)} %maximum_convert_fusion.1, f32[256]{0:T(256)S(1)} %bitcast.159, pred[384]{0:T(512)(128)(4,1)S(1)} %get-tuple-element.110, f32[256]{0:T(256)S(1)} %bitcast.160, pred[384]{0:T(512)(128)(4,1)S(1)} %get-tuple-element.111, ...), kind=kLoop, calls=%fused_computation.286 | loop fusion | flops 9239808 | bytes 12629248 | tf_op jit(solution)/shard_map/reduce_sum | solution.py:102
  246.5 6.5 %all_to_all.32 = f32[4,1,768]{2,1,0:T(1,128)S(1)} all-to-all(f32[4,1,768]{2,1,0:T(1,128)S(1)} %broadcast_in_dim.425), channel_id=1, replica_groups=mesh['sp'=128,'tp'=4] {'tp'}, dimensions={0} | all-to-all | bytes 24576 | tf_op jit(solution)/shard_map/all_to_all | solution.py:28
  253.0 1.9 convolution_convert_fusion
  254.9 1.3 copy.95
  256.2 3.6 %all-to-all-start.4 = ((bf16[4,384,512]{2,1,0:T(8,128)(2,1)}), bf16[4,384,512]{2,1,0:T(8,128)(2,1)S(1)}, u32[]{:S(2)}, u32[]{:S(2)}) async-start(bf16[4,384,512]{2,1,0:T(8,128)(2,1)} %bitcast.139), calls=%async_computation.4 | async-start | bytes 3145728 | tf_op jit(solution)/shard_map/all_to_all | solution.py:52
  260.0 19.1 %all-to-all-done.4 = bf16[4,384,512]{2,1,0:T(8,128)(2,1)S(1)} async-done(((bf16[4,384,512]{2,1,0:T(8,128)(2,1)}), bf16[4,384,512]{2,1,0:T(8,128)(2,1)S(1)}, u32[]{:S(2)}, u32[]{:S(2)}) %all-to-all-start.4) | async-done | bytes 1572896 | tf_op jit(solution)/shard_map/all_to_all | solution.py:52
  279.8 20.8 %all_to_all.33 = bf16[4,384,512]{2,1,0:T(8,128)(2,1)S(1)} all-to-all(bf16[4,384,512]{2,1,0:T(8,128)(2,1)S(1)} %broadcast_in_dim.426), channel_id=1, replica_groups=mesh['sp'=128,'tp'=4] {'tp'}, dimensions={0} | all-to-all | bytes 3145728 | tf_op jit(solution)/shard_map/all_to_all | solution.py:28
  300.6 0.9 copy.72
  301.5 1.6 copy.73
  (43 shorter events, 4.4 us)
Async XLA Ops:
  6.5 153.7 %all-gather.2.cloned.1.call-start = ((), (), s32[]{:S(2)}) async-start(), calls=%async_computation.6 | async-start | bytes 6340608 | tf_op jit(solution)/shard_map/all_gather | solution.py:12
  10.1 10.4 %collective-permute-start.1 = (s32[30]{0:T(128)S(1)}, s32[30]{0:T(128)S(1)}, u32[]{:S(2)}, u32[]{:S(2)}) collective-permute-start(s32[30]{0:T(128)S(1)} %slice.568), channel_id=1, source_target_pairs={{0,4},{4,8},{8,12},{12,16},{16,20},{20,24},{24,28},{28,32},{32,36}... | collective-permute-start | bytes 368 | tf_op jit(solution)/shard_map/ppermute | solution.py:23
  163.8 1.3 copy-start
  163.8 2.6 copy-start.2
  164.0 3.1 copy-start.3
  167.0 2.8 copy-start.5
  167.7 3.1 collective-permute-start
  170.8 8.0 %copy-start.6 = (f32[2,256]{1,0:T(2,128)S(1)}, f32[2,256]{1,0:T(2,128)}, u32[]{:S(2)}) copy-start(f32[2,256]{1,0:T(2,128)} %param.17) | copy-start | bytes 6148
  174.8 8.2 %all-to-all-start = ((f32[4,1,768]{2,1,0:T(1,128)}), f32[4,1,768]{2,1,0:T(1,128)S(1)}, u32[]{:S(2)}, u32[]{:S(2)}) async-start(f32[4,1,768]{2,1,0:T(1,128)} %broadcast_in_dim.423), calls=%async_computation | async-start | bytes 24576 | tf_op jit(solution)/shard_map/all_to_all | solution.py:28
  186.2 22.8 %all-to-all-start.1 = ((bf16[4,384,512]{2,1,0:T(8,128)(2,1)}), bf16[4,384,512]{2,1,0:T(8,128)(2,1)S(1)}, u32[]{:S(2)}, u32[]{:S(2)}) async-start(bf16[4,384,512]{2,1,0:T(8,128)(2,1)} %bitcast.135), calls=%async_computation.1 | async-start | bytes 3145728 | tf_op jit(solution)/shard_map/all_to_all | solution.py:52
  211.7 21.9 %all-to-all-start.2 = ((bf16[4,384,512]{2,1,0:T(8,128)(2,1)}), bf16[4,384,512]{2,1,0:T(8,128)(2,1)S(1)}, u32[]{:S(2)}, u32[]{:S(2)}) async-start(bf16[4,384,512]{2,1,0:T(8,128)(2,1)} %broadcast_in_dim.424), calls=%async_computation.2 | async-start | bytes 3145728 | tf_op jit(solution)/shard_map/all_to_all | solution.py:28
  234.5 1.6 copy-start.1
  235.4 1.7 copy-start.4
  237.8 5.3 %collective-permute-start.2 = (bf16[30,256]{1,0:T(8,128)(2,1)S(1)}, bf16[30,256]{1,0:T(8,128)(2,1)S(1)}, u32[]{:S(2)}, u32[]{:S(2)}) collective-permute-start(bf16[30,256]{1,0:T(8,128)(2,1)S(1)} %slice.775), channel_id=1, source_target_pairs={{0,4},{4,8},{8,12},{12,16},{16,20},{20,24},{24,28},{28,32},{32,36}... | collective-permute-start | bytes 46088 | tf_op jit(solution)/shard_map/ppermute | solution.py:23
  256.2 22.9 %all-to-all-start.4 = ((bf16[4,384,512]{2,1,0:T(8,128)(2,1)}), bf16[4,384,512]{2,1,0:T(8,128)(2,1)S(1)}, u32[]{:S(2)}, u32[]{:S(2)}) async-start(bf16[4,384,512]{2,1,0:T(8,128)(2,1)} %bitcast.139), calls=%async_computation.4 | async-start | bytes 3145728 | tf_op jit(solution)/shard_map/all_to_all | solution.py:52
Sparse Core Ops, SparseCore 0:
  10.5 149.7 all-gather.1
where the time goes:
time: 316 us; the launch traced here: 310 us
  waiting for transfers between devices  197 us (62%)
  blocking collectives  27.3 us (9%)
  local copies, waits for them, and re-layouts  25.7 us (8%)
  starting transfers between devices  25.6 us (8%)
  between operations  13.8 us (4%)
  other arithmetic  13.7 us (4%)
  matrix products  6.31 us (2%)
    all_gather x1, waiting for transfers between devices, rows_first(): out, at, outs = (lax.all_gather(both, axis, axis=0, tiled=True), 0, [])  138 us
    all_to_all x2, waiting for transfers between devices, summed_on_arrival(): lax.all_to_all(pieces, axis, split_axis=0, concat_axis=0, tiled=True)  38.3 us
    all_to_all x2, blocking collectives, sent_to_all(): return lax.all_to_all(copies, axis, split_axis=0, concat_axis=0, tiled=True)  27.3 us
    all_to_all x2, waiting for transfers between devices, sent_to_all(): return lax.all_to_all(copies, axis, split_axis=0, concat_axis=0, tiled=True)  20 us
    ppermute x3, starting transfers between devices, passed_along(): lax.ppermute(value, axis, [(source, source + steps) for source in range(f...  10.9 us
    all_to_all x2, starting transfers between devices, sent_to_all(): return lax.all_to_all(copies, axis, split_axis=0, concat_axis=0, tiled=True)  7.56 us
    all_to_all x2, starting transfers between devices, summed_on_arrival(): lax.all_to_all(pieces, axis, split_axis=0, concat_axis=0, tiled=True)  7.13 us
    reduce_sum x2, other arithmetic, on_device(): jnp.sum(conv_out, axis=1)  6.63 us
  transfers between devices with their start and end apart: 8, of which 6 were waited for; matrix products, arithmetic and copies ran while one was open for 4% of the time, Pallas kernels for 0%

commit v1 on v0

v1 whole, which is shorter than its diff:
```python
import functools

import jax
import jax.numpy as jnp
from jax import lax
from jax.experimental import pallas as pl
from jax.experimental.pallas import tpu as pltpu
from jax.sharding import PartitionSpec as P

EPS = 1e-06
NZ, NX, NC, NY = 16, 4, 2, 4
ROWS, D, C, CB, KW, LAYERS = 384, 2048, 1024, 256, 31, 2
HALO = 32
RB = 128
NB = ROWS // RB
HB = RB // 2
F32, BF16 = jnp.float32, jnp.bfloat16
MESH = pl.DeviceIdType.MESH


def kernel(tok_hbm, docs_ref, gain_ref, v_ref, g_ref, o_ref, taps_ref, ng_ref, ns_ref, out_hbm,
           tok, normed, vg, ot, ag, gs, ge, dx, age, act,
           loc_sem, out_sem, vgx_s, vgx_r, oty_s, oty_r, gsy_s, gsy_r, dx_s, dx_r, halo_s, halo_r,
           vgz_s, vgu_r, vgd_r, otz_s, otu_r, otd_r, otx_s, oxu_r, oxd_r, oxb_r,
           rel_s, rel_r, pv_s, pv_r, po_s, po_r, ag_s, ag_r):
    sp = lax.axis_index("sp")
    y = lax.axis_index("tp")
    z = sp // 8
    x = lax.rem(sp // 2, 4)
    c = lax.rem(sp, 2)

    def at(zz, xx, cc):
        return {"sp": lax.rem(zz + NZ, NZ) * 8 + lax.rem(xx + NX, NX) * 2 + cc}

    def along_y(step):
        return {"tp": lax.rem(y + step + NY, NY)}

    z_up, z_down = at(z + 1, x, c), at(z - 1, x, c)
    x_up, x_down, x_far = at(z, x + 1, c), at(z, x - 1, c), at(z, x + 2, c)
    partner = at(z, x, 1 - c)
    sp_next = {"sp": lax.rem(sp + 1, 128)}
    sp_prev = {"sp": lax.rem(sp + 127, 128)}
    xp, xm, xf = lax.rem(x + 1, NX), lax.rem(x + 3, NX), lax.rem(x + 2, NX)

    def zi(v):
        return lax.rem(v + NZ, NZ)

    def rcopy(src, dst, ssem, rsem, dev):
        return pltpu.make_async_remote_copy(
            src_ref=src, dst_ref=dst, send_sem=ssem, recv_sem=rsem,
            device_id=dev, device_id_type=MESH)

    def push(ref, ssem, rsem, dev):
        rcopy(ref, ref, ssem, rsem, dev).start()

    def sent(ref, ssem):
        rcopy(ref, ref, ssem, ssem, partner).wait_send()

    def got(ref, rsem):
        rcopy(ref, ref, rsem, rsem, partner).wait_recv()

    tok_in = pltpu.make_async_copy(tok_hbm, tok, loc_sem)
    tok_in.start()

    for l in range(LAYERS):
        vg[l, z, x, c, :, 0:CB] = v_ref[l]
        vg[l, z, x, c, :, CB:2 * CB] = g_ref[l]
        ot[l, y, z, x, c] = jnp.transpose(o_ref[l].astype(F32)).astype(BF16)
    gs[y, 0:2, :] = ng_ref[...]
    gs[y, 2:4, :] = ns_ref[...]
    for i in range(3):
        row = jnp.broadcast_to(docs_ref[i:i + 1, :].astype(F32), (128, 128))
        dx[HALO + 128 * i:HALO + 128 * (i + 1), :] = jnp.transpose(row)

    barrier = pltpu.get_barrier_semaphore()
    peers = [z_up, z_down, x_up, x_down, x_far, partner, sp_next, sp_prev,
             along_y(1), along_y(-1), along_y(2)]
    for dev in peers:
        pl.semaphore_signal(barrier, inc=1, device_id=dev, device_id_type=MESH)
    pl.semaphore_wait(barrier, len(peers))

    mine = vg.at[:, z, x, c]
    for i, dev in enumerate((x_up, x_down, x_far)):
        push(mine, vgx_s.at[i], vgx_r.at[i], dev)
    own_o = ot.at[:, y, z, x, c]
    for i, dev in enumerate((along_y(1), along_y(-1), along_y(2))):
        push(own_o, oty_s.at[i], oty_r.at[i], dev)
    for i, dev in enumerate((along_y(1), along_y(-1), along_y(2))):
        push(gs.at[y], gsy_s.at[i], gsy_r.at[i], dev)
    dx_tail, dx_head = dx.at[pl.ds(ROWS, HALO)], dx.at[pl.ds(0, HALO)]
    dx_copy = rcopy(dx_tail, dx_head, dx_s, dx_r, sp_next)
    dx_copy.start()
    for i in range(3):
        got(mine, vgx_r.at[i])

    def vg_part(l, zc, sub):
        return vg.at[l, zc, pl.ds(2 * sub, 2), c]

    def ot_part(l, zc, xx):
        return ot.at[l, :, zc, xx, c]

    def vg_up(l, r, sub):
        push(vg_part(l, zi(z - r), sub), vgz_s.at[l], vgu_r.at[l, sub, r], z_up)

    def vg_down(l, r, sub):
        push(vg_part(l, zi(z + r), sub), vgz_s.at[l], vgd_r.at[l, sub, r], z_down)

    def vg_to_partner(l, zc):
        push(vg.at[l, zc, :, c], pv_s.at[l], pv_r.at[l], partner)

    def ot_up(l, r):
        push(ot_part(l, zi(z - r), x), otz_s.at[l], otu_r.at[l, r], z_up)

    def ot_down(l, r):
        push(ot_part(l, zi(z + r), x), otz_s.at[l], otd_r.at[l, r], z_down)

    def ot_along_x_u(l, r):
        part = ot_part(l, zi(z - r), x)
        push(part, otx_s.at[l], oxu_r.at[l, r], x_up)
        push(part, otx_s.at[l], oxb_r.at[l, 0], x_down)

    def ot_along_x_d(l, r):
        part = ot_part(l, zi(z + r), x)
        push(part, otx_s.at[l], oxd_r.at[l, r], x_down)
        push(part, otx_s.at[l], oxb_r.at[l, 1], x_up)

    def relay_u(l, r):
        part = ot_part(l, zi(z - r), xm)
        got(part, oxu_r.at[l, r])
        push(part, rel_s.at[l], rel_r.at[l, 0], x_up)

    def relay_d(l, r):
        part = ot_part(l, zi(z + r), xp)
        got(part, oxd_r.at[l, r])
        push(part, rel_s.at[l], rel_r.at[l, 1], x_down)

    def first_vg(l):
        for sub in range(2):
            vg_up(l, 0, sub)
            vg_down(l, 0, sub)
        vg_to_partner(l, z)

    def first_ot(l):
        ot_up(l, 0)
        ot_down(l, 0)
        ot_along_x_u(l, 0)

    def middle(l, r):
        for sub in range(2):
            got(vg_part(l, zi(z - r), sub), vgu_r.at[l, sub, r - 1])
            vg_up(l, r, sub)
            got(vg_part(l, zi(z + r), sub), vgd_r.at[l, sub, r - 1])
            vg_down(l, r, sub)
        got(ot_part(l, zi(z - r), x), otu_r.at[l, r - 1])
        ot_up(l, r)
        got(ot_part(l, zi(z + r), x), otd_r.at[l, r - 1])
        ot_down(l, r)
        vg_to_partner(l, zi(z - r))
        vg_to_partner(l, zi(z + r))
        ot_along_x_u(l, r)
        ot_along_x_d(l, r)

    def seventh(l):
        for sub in range(2):
            got(vg_part(l, zi(z - 7), sub), vgu_r.at[l, sub, 6])
            vg_up(l, 7, sub)
            got(vg_part(l, zi(z + 7), sub), vgd_r.at[l, sub, 6])
        got(ot_part(l, zi(z - 7), x), otu_r.at[l, 6])
        ot_up(l, 7)
        got(ot_part(l, zi(z + 7), x), otd_r.at[l, 6])
        vg_to_partner(l, zi(z - 7))
        vg_to_partner(l, zi(z + 7))
        ot_along_x_u(l, 7)
        ot_along_x_d(l, 7)

    def eighth(l):
        for sub in range(2):
            got(vg_part(l, zi(z - 8), sub), vgu_r.at[l, sub, 7])
        vg_to_partner(l, zi(z - 8))
        got(ot_part(l, zi(z - 8), x), otu_r.at[l, 7])
        ot_along_x_u(l, 8)
        push(ot.at[l, :, :, x, c], po_s.at[l], po_r.at[l], partner)

    def relays(l, r):
        relay_u(l, r)
        relay_d(l, r)

    def vg_ready(l):
        got(vg.at[l, :, :, 1 - c], pv_r.at[l])

    def ot_columns(l):
        got(ot.at[l, :, pl.ds(0, 9), xp, c], oxb_r.at[l, 0])
        got(ot.at[l, :, pl.ds(0, 7), xm, c], oxb_r.at[l, 1])
        push(ot.at[l, :, :, xp, c], po_s.at[l], po_r.at[l], partner)
        push(ot.at[l, :, :, xm, c], po_s.at[l], po_r.at[l], partner)
        got(ot.at[l, :, pl.ds(0, 9), xf, c], rel_r.at[l, 0])
        got(ot.at[l, :, pl.ds(0, 7), xf, c], rel_r.at[l, 1])
        push(ot.at[l, :, :, xf, c], po_s.at[l], po_r.at[l], partner)

    def ot_ready(l):
        got(ot.at[l, :, :, :, 1 - c], po_r.at[l])

    first_vg(0)
    for i in range(3):
        got(own_o, oty_r.at[i])
    first_ot(0)

    def normalize(l, start, count):
        wide = tok[pl.ds(start, count), :].astype(F32)
        scale = lax.rsqrt(jnp.mean(wide * wide, axis=-1, keepdims=True) + EPS)
        normed[pl.ds(start, count), :] = (wide * scale * gain_ref[l:l + 1, :]).astype(BF16)

    tok_in.wait()

    @pl.loop(0, ROWS // 32)
    def _(i):
        normalize(0, pl.multiple_of(i * 32, 32), 32)

    dx_copy.wait()
    dx[0:HALO, :] = jnp.where(sp == 0, -1.0, dx[0:HALO, :])
    for b in range(NB):
        here = dx[HALO + b * RB:HALO + (b + 1) * RB, :]
        total = jnp.zeros((RB, 128), F32)
        for j in range(1, KW):
            lo = HALO + b * RB - j
            total = total + jnp.where(dx[lo:lo + RB, :] == here, 1.0, 0.0)
        age[b * RB:(b + 1) * RB, :] = total

    middle(0, 1)
    relay_u(0, 0)

    @pl.loop(2, 7)
    def _(r):
        middle(0, r)
        relays(0, r - 1)

    seventh(0)
    relays(0, 6)
    eighth(0)
    first_vg(1)
    first_ot(1)

    def gate(l):
        @pl.loop(0, NB)
        def _(i):
            start = pl.multiple_of(i * RB, RB)
            both = jnp.dot(normed[pl.ds(start, RB), :], vg[l].reshape(D, 2 * CB),
                           preferred_element_type=F32)
            value = both[:, :CB].astype(BF16).astype(F32)
            gates = both[:, CB:].astype(BF16).astype(F32)
            gated = (value * jax.nn.sigmoid(gates)).astype(BF16).astype(F32)
            for h in range(2):
                ge[l, h, pl.ds(pl.multiple_of(start + HALO, 32), RB), :] = gated[:, 128 * h:128 * (h + 1)]

    def halo_copy(l):
        return rcopy(ge.at[l, :, pl.ds(ROWS, HALO)], ge.at[l, :, pl.ds(0, HALO)],
                     halo_s.at[l], halo_r.at[l], sp_next)

    def conv(l, b):
        for h in range(2):
            lo = HALO + b * RB
            old = age[b * RB:(b + 1) * RB, :]
            lanes = slice(128 * h, 128 * (h + 1))
            total = taps_ref[l, 0:1, lanes] * ge[l, h, lo:lo + RB, :]
            for j in range(1, KW):
                term = taps_ref[l, j:j + 1, lanes] * ge[l, h, lo - j:lo - j + RB, :]
                total = total + jnp.where(old >= j, term, 0.0)
            ag[l, y, b * RB:(b + 1) * RB, lanes] = total.astype(BF16)

    def half(l, who, b, k):
        return ag.at[l, who, pl.ds(b * RB + k * HB, HB)]

    def send_block(l, b):
        push(half(l, y, b, 0), ag_s.at[l], ag_r.at[l, b, 0], along_y(1))
        push(half(l, y, b, 1), ag_s.at[l], ag_r.at[l, b, 3], along_y(-1))
        push(half(l, y, b, 1), ag_s.at[l], ag_r.at[l, b, 1], along_y(1))
        push(half(l, y, b, 0), ag_s.at[l], ag_r.at[l, b, 2], along_y(-1))

    below, above, far = lax.rem(y + 3, NY), lax.rem(y + 1, NY), lax.rem(y + 2, NY)

    def relay_block(l, b):
        got(half(l, below, b, 0), ag_r.at[l, b, 0])
        push(half(l, below, b, 0), ag_s.at[l], ag_r.at[l, b, 4], along_y(1))
        got(half(l, above, b, 1), ag_r.at[l, b, 3])
        push(half(l, above, b, 1), ag_s.at[l], ag_r.at[l, b, 5], along_y(-1))

    def block_ready(l, b):
        got(half(l, below, b, 1), ag_r.at[l, b, 1])
        got(half(l, above, b, 0), ag_r.at[l, b, 2])
        got(half(l, far, b, 0), ag_r.at[l, b, 4])
        got(half(l, far, b, 1), ag_r.at[l, b, 5])

    def activate(l, b):
        @pl.loop(0, RB // 32)
        def _(i):
            rows = pl.ds(pl.multiple_of(b * RB + i * 32, 32), 32)
            parts = [ag[l, k, rows, :].astype(F32) for k in range(NY)]
            mean = sum(jnp.sum(p, axis=-1, keepdims=True) for p in parts) * (1.0 / C)
            parts = [p - mean for p in parts]
            var = sum(jnp.sum(p * p, axis=-1, keepdims=True) for p in parts) * (1.0 / C)
            scale = lax.rsqrt(var + EPS)
            for k in range(NY):
                n = gs[k, l:l + 1, :] * parts[k] * scale + gs[k, 2 + l:3 + l, :]
                act[k, pl.ds(pl.multiple_of(i * 32, 32), 32), :] = (n * jax.nn.sigmoid(n)).astype(BF16)

    def project(l, b):
        @pl.loop(0, 4)
        def _(n):
            total = jnp.zeros((RB, 512), F32)
            for k in range(NY):
                weights = ot[l, k, pl.ds(n * 4, 4)].reshape(512, CB)
                total = total + lax.dot_general(act[k], weights, (((1,), (1,)), ((), ())),
                                                preferred_element_type=F32)
            cols = pl.ds(pl.multiple_of(n * 512, 512), 512)
            rows = pl.ds(b * RB, RB)
            tok[rows, cols] = (tok[rows, cols].astype(F32)
                               + total.astype(BF16).astype(F32)).astype(BF16)

    order = tuple(reversed(range(NB)))

    def layer(l, steps):
        steps = list(steps)

        def step():
            if steps:
                steps.pop(0)()

        gate(l)
        copy = halo_copy(l)
        copy.start()
        step()
        for n, b in enumerate(order):
            if b == 0:
                copy.wait()
                ge[l, :, 0:HALO, :] = jnp.where(sp == 0, 0.0, ge[l, :, 0:HALO, :])
            conv(l, b)
            send_block(l, b)
            if n:
                relay_block(l, order[n - 1])
        step()
        relay_block(l, order[-1])
        step()
        for n, b in enumerate(order):
            block_ready(l, b)
            activate(l, b)
            if n == 0:
                ot_columns(l)
                ot_ready(l)
            project(l, b)
            if l + 1 < LAYERS:
                @pl.loop(0, RB // 32)
                def _(i):
                    normalize(l + 1, pl.multiple_of(b * RB + i * 32, 32), 32)
            else:
                out_copy(b).start()
            step()
        while steps:
            step()

    def out_copy(b):
        rows = pl.ds(b * RB, RB)
        return pltpu.make_async_copy(tok.at[rows], out_hbm.at[rows], out_sem.at[b])

    def later_step(r):
        def run():
            if r == 7:
                seventh(1)
            elif r == 8:
                eighth(1)
            else:
                middle(1, r)
            relay_u(1, r - 1)
            if r > 1:
                relay_d(1, r - 1)
            if r == 8:
                relay_u(1, 8)
        return run

    for i in range(3):
        got(gs.at[y], gsy_r.at[i])
    relays(0, 7)
    relay_u(0, 8)
    vg_ready(0)
    layer(0, [later_step(r) for r in range(1, 9)])
    vg_ready(1)
    layer(1, [])

    for b in range(NB):
        out_copy(b).wait()
    for i in range(3):
        sent(mine, vgx_s.at[i])
        sent(own_o, oty_s.at[i])
        sent(gs.at[y], gsy_s.at[i])
    for l in range(LAYERS):
        sent(vg.at[l, pl.ds(0, 15), :, c], vgz_s.at[l])
        sent(vg.at[l, :, :, c], pv_s.at[l])
        sent(ot.at[l, :, pl.ds(0, 15), x, c], otz_s.at[l])
        sent(ot.at[l, :, :, pl.ds(0, 2), c], otx_s.at[l])
        sent(ot.at[l, :, :, 0, c], rel_s.at[l])
        sent(ot.at[l, :, :, :, c], po_s.at[l])
        sent(ag.at[l, pl.ds(0, 3)], ag_s.at[l])


def on_device(tokens, doc_ids, pre_gain, value_proj, gate_proj, out_proj, conv_taps, norm_gain, norm_shift):
    vmem = pl.BlockSpec(memory_space=pltpu.VMEM)
    hbm = pl.BlockSpec(memory_space=pl.ANY)
    dma = pltpu.SemaphoreType.DMA
    L = LAYERS
    return pl.pallas_call(
        kernel,
        out_shape=jax.ShapeDtypeStruct((ROWS, D), BF16),
        in_specs=[hbm] + [vmem] * 8,
        out_specs=hbm,
        scratch_shapes=[
            pltpu.VMEM((ROWS, D), BF16),
            pltpu.VMEM((ROWS, D), BF16),
            pltpu.VMEM((L, NZ, NX, NC, 16, 2 * CB), BF16),
            pltpu.VMEM((L, NY, NZ, NX, NC, 16, CB), BF16),
            pltpu.VMEM((L, NY, ROWS, CB), BF16),
            pltpu.VMEM((NY, 8, CB), F32),
            pltpu.VMEM((L, 2, HALO + ROWS, 128), F32),
            pltpu.VMEM((HALO + ROWS, 128), F32),
            pltpu.VMEM((ROWS, 128), F32),
            pltpu.VMEM((NY, RB, CB), BF16),
            dma(()), dma((NB,)),
            dma((3,)), dma((3,)), dma((3,)), dma((3,)), dma((3,)), dma((3,)),
            dma(()), dma(()), dma((L,)), dma((L,)),
            dma((L,)), dma((L, 2, 8)), dma((L, 2, 7)),
            dma((L,)), dma((L, 8)), dma((L, 7)),
            dma((L,)), dma((L, 9)), dma((L, 8)), dma((L, 2)),
            dma((L,)), dma((L, 2)),
            dma((L,)), dma((L,)), dma((L,)), dma((L,)),
            dma((L,)), dma((L, NB, 6)),
        ],
        compiler_params=pltpu.CompilerParams(
            collective_id=0, has_side_effects=True, vmem_limit_bytes=48 * 1024 * 1024),
    )(tokens, doc_ids.reshape(3, 128), pre_gain, value_proj, gate_proj, out_proj,
      conv_taps, norm_gain, norm_shift)


def solution(mesh):
    return jax.shard_map(
        on_device,
        mesh=mesh,
        in_specs=(
            P("sp", None),
            P("sp"),
            P(),
            P(None, "sp", "tp"),
            P(None, "sp", "tp"),
            P(None, "tp", "sp"),
            P(None, None, "tp"),
            P(None, "tp"),
            P(None, "tp"),
        ),
        out_specs=P("sp", None),
        check_vma=False,
    )
```

time: 316 us -> 117 us (0.37); the launches traced: 310 us -> 116 us
  waiting for transfers between devices: 197 us -> 0 us
  Pallas kernels: 0 us -> 108 us
  blocking collectives: 27.3 us -> 0 us
  starting transfers between devices: 25.6 us -> 0 us
  local copies, waits for them, and re-layouts: 25.7 us -> 8.42 us
  between operations: 13.8 us -> 0.03 us
  other arithmetic: 13.7 us -> 0 us
  matrix products: 6.31 us -> 0 us
    all_gather x1 -> x0, waiting for transfers between devices: 138 us -> none  [rows_first(): out, at, outs = (lax.all_gather(both, axis, axis=0, tiled=True), 0, [])]
    pallas_call x0 -> x1, Pallas kernels: none -> 108 us  [on_device(): pl.pallas_call(kernel, out_shape=jax.ShapeDtypeStruct((ROWS, D), BF16), i...]
    all_to_all x4 -> x0, waiting for transfers between devices: 58.3 us -> none  [the longest x2 38.3 us: summed_on_arrival(): lax.all_to_all(pieces, axis, split_axis=0, concat_axis=0, tiled=True)]
    all_to_all x2 -> x0, blocking collectives: 27.3 us -> none  [sent_to_all(): return lax.all_to_all(copies, axis, split_axis=0, concat_axis=0, tiled=True)]
    all_to_all x4 -> x0, starting transfers between devices: 14.7 us -> none  [the longest x2 7.56 us: sent_to_all(): return lax.all_to_all(copies, axis, split_axis=0, concat_axis=0, tiled=True)]
    ppermute x3 -> x0, starting transfers between devices: 10.9 us -> none  [passed_along(): lax.ppermute(value, axis, [(source, source + steps) for source in range(f...]
    reduce_sum x8 -> x0, other arithmetic: 9.76 us -> none  [the longest x2 6.63 us: on_device(): jnp.sum(conv_out, axis=1)]
    slice x11 -> x0, local copies, waits for them, and re-layouts: 9.17 us -> none  [the longest x1 3.42 us: rows_first(): slab = out[:, at:at + t[0].size].reshape(-1, *t.shape[1:])]
  transfers between devices with their start and end apart: 8 -> 0, of which waited for: 6 -> 0; matrix products, arithmetic and copies ran while one was open for 4% -> 0% of each run, Pallas kernels for 0% -> 0%
where the time goes in v1:
time: 117 us; the launch traced here: 116 us
  Pallas kernels  108 us (92%)
  local copies, waits for them, and re-layouts  8.42 us (7%)
    pallas_call x1, Pallas kernels, on_device(): pl.pallas_call(kernel, out_shape=jax.ShapeDtypeStruct((ROWS, D), BF16), i...  108 us
    unnamed x17, local copies, waits for them, and re-layouts  8.42 us

profile of v1, /device:TPU:1, one launch (start us, length us, event | category | flops | bytes accessed | tf_op | source)
XLA Modules:
  0.0 116.5 jit_solution(16259004310760546806)
XLA Ops:
  0.0 0.8 copy.11.taps_ref
  0.8 0.8 copy.10.o_ref
  1.7 0.0 copy-start
  1.7 1.4 %copy-done = bf16[384,2048]{1,0:T(8,128)(2,1)S(1)} copy-done((bf16[384,2048]{1,0:T(8,128)(2,1)S(1)}, bf16[384,2048]{1,0:T(8,128)(2,1)}, u32[]{:S(2)}) %copy-start) | copy-done | bytes 1572888
  3.1 0.0 copy-start.1
  3.1 0.7 copy-done.1
  3.8 0.0 copy-start.2
  3.8 0.7 copy-done.2
  4.5 0.0 copy-start.3
  4.5 0.7 copy-done.3
  5.2 0.0 copy-start.4
  5.2 0.7 copy-done.4
  5.9 0.0 copy-start.5
  5.9 0.7 copy-done.5
  6.6 0.0 copy-start.6
  6.6 0.7 copy-done.6
  7.3 108.0 %shard_map.91 = bf16[384,2048]{1,0:T(8,128)(2,1)S(1)} custom-call(bf16[384,2048]{1,0:T(8,128)(2,1)S(1)} %copy-done, s32[3,128]{1,0:T(4,128)S(1)} %bitcast.1, f32[2,2048]{1,0:T(2,128)S(1)} %copy-done.1, bf16[2,16,256]{2,1,0:T(8,128)(2,1)S(1)} %copy-done.2, bf16[2,16,256]{2,1,0:T(8,128)(2,1)S(1)} %copy-done.3, bf16[2,256,16]{2,1,0:T(8,128)(2,1)S(1)} %copy.10.o_ref, ...), custom_call_target="tpu_custom_call" | custom-call | tf_op jit(solution)/shard_map/pallas_call | solution.py:409
  115.3 1.1 copy.13
Async XLA Ops:
  1.7 1.4 %copy-start = (bf16[384,2048]{1,0:T(8,128)(2,1)S(1)}, bf16[384,2048]{1,0:T(8,128)(2,1)}, u32[]{:S(2)}) copy-start(bf16[384,2048]{1,0:T(8,128)(2,1)} %tok_hbm.1) | copy-start | bytes 4718596
  3.1 0.7 copy-start.1
  3.8 0.7 copy-start.2
  4.5 0.7 copy-start.3
  5.2 0.7 copy-start.4
  5.9 0.7 copy-start.5
  6.6 0.7 copy-start.6
